TPU v7x, 32 devices: a whole 2x2x4 slice. The times are simulated.
32 devices in a mesh: sp: 4 (over y, x), tp: 8 (over z, core).
Axes of the slice: x: 2, y: 2, z: 4, core: 2. Of those that a mesh axis runs over, the one named last changes fastest.
Arguments:
- stream: bfloat16 [8, 1536, 2048], P('tp', 'sp'), may hold values from -80 to 80
- norm_gain: float32 [2048], replicated, may hold values from 0.1 to 1.9
- w_lin: bfloat16 [1024, 2048], P('tp'), may hold values from -0.125 to 0.125
- w_gate: bfloat16 [1024, 2048], P('tp'), may hold values from -0.125 to 0.125
- conv_taps: bfloat16 [31, 1024], replicated, may hold values from -3 to 3
- conv_bias: float32 [1024], replicated, may hold values from -3 to 3
- ln_gain: float32 [1024], replicated, may hold values from 0.1 to 1.9
- ln_shift: float32 [1024], replicated, may hold values from -3 to 3
- w_proj: bfloat16 [1024, 2048], P('tp'), may hold values from -0.1875 to 0.1875
Outputs:
- result_stream: bfloat16 [8, 1536, 2048], P('tp', 'sp')
All inputs are finite; a program needn't handle non-finite values.
Results may differ from a plain program's by a relative error of at most 0.0024.
Values may be sent and summed in bfloat16 or wider, within the bound.
No kernel may reach another device: no remote copies, remote signals or barrier semaphores. Data moves between devices by JAX's collectives and lax.ppermute only.
A program may use at most 64 MiB of HBM per device.

v0:
```python
import jax
import jax.numpy as jnp
from jax import lax
from jax.sharding import PartitionSpec as P

KW = 31


EPS = 1e-06


def passed_along(value, axis, steps):
    count = lax.axis_size(axis)
    leading, last = (max(0, -steps), min(count, count - steps))
    return lax.ppermute(value, axis, [(source, source + steps) for source in range(leading, last)])


def rms_rows(rows, gain):
    full = rows.astype(jnp.float32)
    scale = lax.rsqrt(jnp.mean(full * full, axis=1, keepdims=True) + EPS)
    return (full * scale * gain).astype(jnp.bfloat16)


def local(stream, norm_gain, w_lin, w_gate, conv_taps, conv_bias, ln_gain, ln_shift, w_proj):
    rows = stream.shape[1]
    reach = KW - 1
    current = stream[0]
    normed = rms_rows(current, norm_gain)
    paired = jnp.stack([w_lin, w_gate], axis=1)
    both = jnp.einsum(
        "td,nrd->trn",
        normed,
        lax.all_gather(paired, "tp", axis=0, tiled=True),
        preferred_element_type=jnp.float32,
    )
    linear = both[:, 0]
    gating = both[:, 1]
    mixed = (linear * jax.nn.sigmoid(gating)).astype(jnp.bfloat16)
    earlier_mixed = passed_along(mixed[rows - reach :], "sp", 1)
    padded = jnp.concatenate([earlier_mixed, mixed], axis=0).astype(jnp.float32)
    taps_full = conv_taps.astype(jnp.float32)
    conv = jnp.zeros((rows, mixed.shape[1]), jnp.float32)
    for tap in range(KW):
        conv = conv + taps_full[tap] * padded[tap : tap + rows]
    conv = conv + conv_bias
    mean = jnp.mean(conv, axis=1, keepdims=True)
    meansq = jnp.mean(conv * conv, axis=1, keepdims=True)
    var = meansq - mean * mean
    activated = jax.nn.silu((conv - mean) * lax.rsqrt(var + EPS) * ln_gain + ln_shift).astype(
        jnp.bfloat16
    )
    projected = jnp.dot(
        activated,
        lax.all_gather(w_proj, "tp", axis=0, tiled=True),
        preferred_element_type=jnp.float32,
    )
    return (current.astype(jnp.float32) + projected).astype(jnp.bfloat16)[None]


def solution(mesh):
    placed = (
        P("tp", "sp", None),
        P(),
        P("tp", None),
        P("tp", None),
        P(),
        P(),
        P(),
        P(),
        P("tp", None),
    )
    return jax.shard_map(
        local, mesh=mesh, in_specs=placed, out_specs=P("tp", "sp", None), check_vma=False
    )
```

profile of v0, /device:TPU:21, one launch (start us, length us, event | category | flops | bytes accessed | tf_op | source)
XLA Modules:
  0.0 150.7 jit_solution(13134745688078922933)
XLA Ops:
  6.5 0.0 all-gather.3.cloned.1.call-start
  6.5 0.0 copy-start
  6.5 2.4 %pad_maximum_fusion = bf16[128,2,2048]{2,0,1:T(8,128)(2,1)} fusion(bf16[128,1,2048]{2,0,1:T(8,128)(2,1)} %bitcast.54, bf16[128,1,2048]{2,0,1:T(8,128)(2,1)} %bitcast.55), kind=kLoop, calls=%fused_computation.83 | loop fusion | flops 524288 | bytes 2097152 | tf_op jit(solution)/shard_map/stack | solution.py:29
  8.9 0.0 copy-start.1
  8.9 0.0 copy-start.3
  8.9 0.0 all-gather.3.cloned.1.call-update
  9.0 0.0 all-gather.5.cloned.1.call-start
  9.0 0.7 all-gather.5.cloned.1.call-update
  9.7 0.0 copy-done
  9.7 0.4 fusion
  10.1 0.0 copy-done.1
  10.2 0.1 fusion.54
  10.2 80.8 %all-gather.3.cloned.1.call-done = bf16[1024,2,2048]{2,0,1:T(8,128)(2,1)} async-done(((bf16[128,2,2048]{2,0,1:T(8,128)(2,1)}), bf16[1024,2,2048]{2,0,1:T(8,128)(2,1)}) %all-gather.3.cloned.1.call-update) | async-done | bytes 8388624 | tf_op jit(solution)/shard_map/all_gather | solution.py:33
  91.1 0.0 copy-done.3
  91.1 5.9 %convolution_bitcast_fusion = f32[384,2,1024]{2,0,1:T(8,128)S(1)} fusion(bf16[1024,2,2048]{2,0,1:T(8,128)(2,1)} %all-gather.3.cloned.1.call-done, bf16[1,384,2048]{2,1,0:T(8,128)(2,1)S(1)} %copy-done, f32[2048]{0:T(1024)S(1)} %copy-done.3, f32[384]{0:T(512)S(1)} %add_rsqrt_fusion.1), kind=kOutput, calls=%fused_computation.8 | convolution fusion | flops 3224371200 | bytes 13116928 | tf_op jit(solution)/shard_map/td,nrd->trn/dot_general | solution.py:30
  97.0 0.4 fusion.45
  97.4 3.1 %collective-permute-start = (bf16[30,1024]{1,0:T(8,128)(2,1)S(1)}, bf16[30,1024]{1,0:T(8,128)(2,1)S(1)}, u32[]{:S(2)}, u32[]{:S(2)}) collective-permute-start(bf16[30,1024]{1,0:T(8,128)(2,1)S(1)} %slice_bitcast_fusion), channel_id=1, source_target_pairs={{0,8},{8,16},{16,24},{1,9},{9,17},{17,25},{2,10},{10,18},{18,26},{... | collective-permute-start | bytes 184328 | tf_op jit(solution)/shard_map/ppermute | solution.py:15
  100.5 0.4 fusion.58
  101.0 0.0 copy-start.2
  101.0 2.8 %collective-permute-done = bf16[30,1024]{1,0:T(8,128)(2,1)S(1)} collective-permute-done((bf16[30,1024]{1,0:T(8,128)(2,1)S(1)}, bf16[30,1024]{1,0:T(8,128)(2,1)S(1)}, u32[]{:S(2)}, u32[]{:S(2)}) %collective-permute-start) | collective-permute-done | bytes 61472 | tf_op jit(solution)/shard_map/ppermute | solution.py:15
  103.7 0.2 maximum_convert_fusion
  104.0 0.0 copy-done.2
  104.0 0.0 copy-start.4
  104.0 0.0 copy-start.5
  104.0 7.5 %fusion.52 = (f32[384]{0:T(512)S(1)}, f32[384]{0:T(512)S(1)}, f32[384,1024]{1,0:T(8,128)S(1)}) fusion(f32[1024]{0:T(1024)S(1)} %copy-done.2, f32[414,1024]{1,0:T(8,128)S(1)} %maximum_convert_fusion, f32[1024]{0:T(1024)S(1)} %bitcast.67, f32[1024]{0:T(1024)S(1)} %bitcast.66, f32[1024]{0:T(1024)S(1)} %bitcast.65, f32[1024]{0:T(1024)S(1)} %bitcast.64, ...), kind=kLoop, calls=%fused_computation.95 | loop fusion | flops 25558272 | bytes 50465792 | tf_op jit(solution)/shard_map/reduce_sum | solution.py:46
  111.6 26.8 %all-gather.5.cloned.1.call-done = bf16[1024,2048]{1,0:T(8,128)(2,1)} async-done(((bf16[128,2048]{1,0:T(8,128)(2,1)}), bf16[1024,2048]{1,0:T(8,128)(2,1)}) %all-gather.5.cloned.1.call-update) | async-done | bytes 4194320 | tf_op jit(solution)/shard_map/all_gather | solution.py:54
  138.4 0.0 copy-done.4
  138.4 0.0 copy-done.5
  138.4 5.5 %fusion.4 = bf16[1,384,2048]{2,1,0:T(8,128)(2,1)} fusion(bf16[1024,2048]{1,0:T(8,128)(2,1)} %all-gather.5.cloned.1.call-done, bf16[1,384,2048]{2,1,0:T(8,128)(2,1)S(1)} %copy-done, f32[384,1024]{1,0:T(8,128)S(1)} %get-tuple-element.7, f32[1024]{0:T(1024)S(1)} %copy-done.4, f32[1024]{0:T(1024)S(1)} %copy-done.5, f32[384]{0:T(512)S(1)} %get-tuple-element.40, ...), kind=kOutput, calls=%fused_computation.7 | convolution fusion | flops 1616510976 | bytes 8924160 | tf_op jit(solution)/shard_map/dot_general | solution.py:52
  (4 shorter events, 0.1 us)
Async XLA Ops:
  6.5 84.5 %all-gather.3.cloned.1.call-start = ((), (), s32[]{:S(2)}) async-start(), calls=%async_computation | async-start | bytes 9437184 | tf_op jit(solution)/shard_map/all_gather | solution.py:33
  6.5 3.2 %copy-start = (bf16[1,384,2048]{2,1,0:T(8,128)(2,1)S(1)}, bf16[1,384,2048]{2,1,0:T(8,128)(2,1)}, u32[]{:S(2)}) copy-start(bf16[1,384,2048]{2,1,0:T(8,128)(2,1)} %param.9) | copy-start | bytes 4718596
  8.9 1.2 copy-start.1
  8.9 82.1 %copy-start.3 = (f32[2048]{0:T(1024)S(1)}, f32[2048]{0:T(1024)}, u32[]{:S(2)}) copy-start(f32[2048]{0:T(1024)} %param.10) | copy-start | bytes 24580
  9.0 129.4 %all-gather.5.cloned.1.call-start = ((), (), s32[]{:S(2)}) async-start(), calls=%async_computation.1 | async-start | bytes 4718592 | tf_op jit(solution)/shard_map/all_gather | solution.py:54
  97.4 6.3 %collective-permute-start = (bf16[30,1024]{1,0:T(8,128)(2,1)S(1)}, bf16[30,1024]{1,0:T(8,128)(2,1)S(1)}, u32[]{:S(2)}, u32[]{:S(2)}) collective-permute-start(bf16[30,1024]{1,0:T(8,128)(2,1)S(1)} %slice_bitcast_fusion), channel_id=1, source_target_pairs={{0,8},{8,16},{16,24},{1,9},{9,17},{17,25},{2,10},{10,18},{18,26},{... | collective-permute-start | bytes 184328 | tf_op jit(solution)/shard_map/ppermute | solution.py:15
  101.0 3.0 %copy-start.2 = (f32[1024]{0:T(1024)S(1)}, f32[1024]{0:T(1024)}, u32[]{:S(2)}) copy-start(f32[1024]{0:T(1024)} %param.14) | copy-start | bytes 12292
  104.0 34.4 %copy-start.4 = (f32[1024]{0:T(1024)S(1)}, f32[1024]{0:T(1024)}, u32[]{:S(2)}) copy-start(f32[1024]{0:T(1024)} %param.16) | copy-start | bytes 12292
  104.0 34.4 %copy-start.5 = (f32[1024]{0:T(1024)S(1)}, f32[1024]{0:T(1024)}, u32[]{:S(2)}) copy-start(f32[1024]{0:T(1024)} %param.15) | copy-start | bytes 12292
Sparse Core Ops, SparseCore 0:
  9.1 81.9 all-gather.2
  92.7 45.6 all-gather.4
where the time goes:
time: 153 us; the launch traced here: 151 us
  waiting for transfers between devices  111 us (73%)
  between operations  13.5 us (9%)
  other arithmetic  11.4 us (7%)
  matrix products  11.4 us (7%)
  starting transfers between devices  3.15 us (2%)
    all_gather x1, waiting for transfers between devices, local(): lax.all_gather(paired, 'tp', axis=0, tiled=True)  80.8 us
    all_gather x1, waiting for transfers between devices, local(): lax.all_gather(w_proj, 'tp', axis=0, tiled=True)  26.8 us
    reduce_sum x1, other arithmetic, local(): mean = jnp.mean(conv, axis=1, keepdims=True)  7.54 us
    dot_general x1, matrix products, local(): jnp.einsum('td,nrd->trn', normed, lax.all_gather(paired, 'tp', axis=0, ti...  5.89 us
    dot_general x1, matrix products, local(): jnp.dot(activated, lax.all_gather(w_proj, 'tp', axis=0, tiled=True), pref...  5.54 us
    ppermute x1, starting transfers between devices, passed_along(): lax.ppermute(value, axis, [(source, source + steps) for source in range(l...  3.11 us
  transfers between devices with their start and end apart: 3, of which 3 were waited for; matrix products, arithmetic and copies ran while one was open for 10% of the time, Pallas kernels for 0%

commit v1 on v0

v1 whole, which is shorter than its diff:
```python
import functools

import jax
import jax.numpy as jnp
from jax import lax
from jax.experimental import pallas as pl
from jax.experimental.pallas import tpu as pltpu
from jax.sharding import PartitionSpec as P

KW = 31
REACH = KW - 1
HALO = 32
EPS = 1e-06
F32 = jnp.float32
BF16 = jnp.bfloat16
VMEM = pl.BlockSpec(memory_space=pltpu.VMEM)


def rms_rows(rows, gain):
    full = rows.astype(F32)
    scale = lax.rsqrt(jnp.mean(full * full, axis=1, keepdims=True) + EPS)
    return (full * scale * gain).astype(BF16)


def passed_along(value, axis, steps):
    count = lax.axis_size(axis)
    leading, last = (max(0, -steps), min(count, count - steps))
    return lax.ppermute(value, axis, [(source, source + steps) for source in range(leading, last)])


def plain(stream, norm_gain, w_lin, w_gate, conv_taps, conv_bias, ln_gain, ln_shift, w_proj):
    rows = stream.shape[1]
    current = stream[0]
    normed = rms_rows(current, norm_gain)
    paired = jnp.stack([w_lin, w_gate], axis=1)
    both = jnp.einsum(
        "td,nrd->trn",
        normed,
        lax.all_gather(paired, "tp", axis=0, tiled=True),
        preferred_element_type=F32,
    )
    mixed = (both[:, 0] * jax.nn.sigmoid(both[:, 1])).astype(BF16)
    earlier_mixed = passed_along(mixed[rows - REACH :], "sp", 1)
    padded = jnp.concatenate([earlier_mixed, mixed], axis=0).astype(F32)
    taps_full = conv_taps.astype(F32)
    conv = jnp.zeros((rows, mixed.shape[1]), F32)
    for tap in range(KW):
        conv = conv + taps_full[tap] * padded[tap : tap + rows]
    conv = conv + conv_bias
    mean = jnp.mean(conv, axis=1, keepdims=True)
    meansq = jnp.mean(conv * conv, axis=1, keepdims=True)
    var = meansq - mean * mean
    activated = jax.nn.silu((conv - mean) * lax.rsqrt(var + EPS) * ln_gain + ln_shift).astype(BF16)
    projected = jnp.dot(
        activated, lax.all_gather(w_proj, "tp", axis=0, tiled=True), preferred_element_type=F32
    )
    return (current.astype(F32) + projected).astype(BF16)[None]


def piece_kernel(normed, mine, other, taps, bias, conv, mixed):
    rows, lanes = conv.shape
    half = lanes // 2
    hidden = normed[...]
    contract = (((1,), (1,)), ((), ()))
    for side, weights in enumerate((mine, other)):
        linear = lax.dot_general(hidden, weights[0], contract, preferred_element_type=F32)
        gating = lax.dot_general(hidden, weights[1], contract, preferred_element_type=F32)
        gated = (linear * jax.nn.sigmoid(gating)).astype(BF16)
        mixed[:, side * half : (side + 1) * half] = gated.astype(F32)
    block = 64
    for lane in range(0, lanes, 128):
        cols = pl.ds(lane, 128)
        for row in range(0, rows, block):
            total = jnp.broadcast_to(bias[0:1, cols], (block, 128))
            for low in range(8):
                reach = block + 24
                first = row + low + HALO - REACH
                reach = min(reach, mixed.shape[0] - first)
                window = mixed[pl.ds(first, reach), cols]
                for high in range(4):
                    tap = 8 * high + low
                    if tap < KW:
                        total += taps[tap : tap + 1, cols] * window[8 * high : 8 * high + block]
            conv[pl.ds(row, block), cols] = total


def piece(normed, mine, other, taps, bias):
    rows = normed.shape[0] - HALO
    lanes = 2 * mine.shape[1]
    flops = 4 * normed.shape[0] * normed.shape[1] * lanes
    return pl.pallas_call(
        piece_kernel,
        out_shape=jax.ShapeDtypeStruct((rows, lanes), F32),
        in_specs=[VMEM] * 5,
        out_specs=VMEM,
        scratch_shapes=[pltpu.VMEM((normed.shape[0], lanes), F32)],
        compiler_params=pltpu.CompilerParams(vmem_limit_bytes=24 * 2**20),
        cost_estimate=pl.CostEstimate(flops=flops, bytes_accessed=0, transcendentals=0),
    )(normed, mine, other, taps, bias)


def finish_kernel(count, current, gain, shift, *refs):
    convs, weights, out = refs[:count], refs[count:-1], refs[-1]
    lanes = convs[0].shape[1]
    channels = count * lanes
    total = sum(jnp.sum(c[...], axis=1, keepdims=True) for c in convs)
    square = sum(jnp.sum(c[...] * c[...], axis=1, keepdims=True) for c in convs)
    mean = total / channels
    var = square / channels - mean * mean
    scale = lax.rsqrt(var + EPS)
    projected = current[...].astype(F32)
    for k, c in enumerate(convs):
        y = (c[...] - mean) * scale * gain[k : k + 1] + shift[k : k + 1]
        act = (y * jax.nn.sigmoid(y)).astype(BF16)
        half = lanes // 2
        for side in range(2):
            projected += jnp.dot(
                act[:, side * half : (side + 1) * half], weights[2 * k + side][...], preferred_element_type=F32
            )
    out[...] = projected.astype(BF16)


def finish(current, gain, shift, convs, weights):
    rows, width = current.shape
    return pl.pallas_call(
        functools.partial(finish_kernel, len(convs)),
        out_shape=jax.ShapeDtypeStruct((rows, width), BF16),
        in_specs=[VMEM] * (3 + len(convs) + len(weights)),
        out_specs=VMEM,
        compiler_params=pltpu.CompilerParams(vmem_limit_bytes=32 * 2**20),
        cost_estimate=pl.CostEstimate(
            flops=2 * rows * width * len(convs) * convs[0].shape[1], bytes_accessed=0, transcendentals=0
        ),
    )(current, gain, shift, *convs, *weights)


def send(value, label, target):
    ways, both = lax.axis_size("sp"), lax.axis_size("tp")
    pairs = []
    for q in range(ways):
        for z in range(both // 2):
            for c in range(2):
                t = target(q, z, c)
                if t is not None:
                    pairs.append((q * both + z * 2 + c, t[0] * both + t[1] * 2 + t[2]))
    with jax.named_scope(label):
        return lax.ppermute(value, ("sp", "tp"), pairs)


def to_plane_first(q, z, c):
    return (q ^ (1 + c), z, c)


def to_plane_second(q, z, c):
    return (q ^ (2 - c), z, c)


def to_other_core(q, z, c):
    return (q, z, 1 - c)


def put(base, value, at):
    return lax.dynamic_update_slice_in_dim(base, value, at, 1)


def spread(value, label, q, c):
    r = value.shape[1]
    first, second = 1 + c, 2 - c
    p1 = send(value, "xa" + label, to_plane_first)
    two = jnp.concatenate([value, p1], axis=1)
    p2 = send(two, "xb" + label, to_plane_second)
    whole = jnp.zeros((value.shape[0], 4 * r, value.shape[2]), value.dtype)
    whole = put(whole, value, q * r)
    whole = put(whole, p1, (q ^ first) * r)
    whole = put(whole, p2[:, :r], (q ^ second) * r)
    return put(whole, p2[:, r:], (q ^ 3) * r)


def fast(stream, norm_gain, w_lin, w_gate, conv_taps, conv_bias, ln_gain, ln_shift, w_proj):
    current = stream[0]
    rows = current.shape[0]
    q, me = lax.axis_index("sp"), lax.axis_index("tp")
    z, c = me // 2, me % 2
    depth = lax.axis_size("tp") // 2
    shard = w_lin.shape[0]
    quarter = shard // lax.axis_size("sp")

    def cut(w):
        return lax.dynamic_slice_in_dim(w, q * quarter, quarter, 0)

    hops = [k for k in (1, 3, 2)]
    gates = jnp.stack([cut(w_lin), cut(w_gate)])
    far_gates = {k: send(gates, f"zg{k}", lambda q, z, c, k=k: (q, z ^ k, c)) for k in hops}
    ways = lax.axis_size("sp")
    earlier = send(current[rows - HALO :], "halo", lambda q, z, c: (q + 1, z, c) if q + 1 < ways else None)
    own_gates = jnp.stack([w_lin, w_gate])
    other_gates = send(own_gates, "dg0", to_other_core)
    other_proj = send(w_proj, "dp0", to_other_core)
    proj = cut(w_proj)
    far_proj = {k: send(proj, f"zp{k}", lambda q, z, c, k=k: (q, z ^ k, c)) for k in hops}

    normed = jnp.concatenate([rms_rows(earlier, norm_gain), rms_rows(current, norm_gain)], axis=0)

    def by_piece(p):
        p = p.astype(F32).reshape(-1, depth, 2 * shard)
        swapped = jnp.concatenate([p[:, :, shard:], p[:, :, :shard]], axis=2)
        return jnp.where(c == 0, p, swapped).transpose(1, 0, 2)

    taps = by_piece(conv_taps)
    small = by_piece(jnp.stack([conv_bias, ln_gain, ln_shift]))
    order = [0] + hops

    def of(p, k):
        return lax.dynamic_index_in_dim(p, z ^ k, 0, keepdims=False)

    params = [of(small, k) for k in order]
    convs = []
    for k, s in zip(order, params):
        if k == 0:
            mine, other = own_gates, other_gates
        else:
            mine = spread(far_gates[k], f"g{k}", q, c)
            other = send(mine, f"dg{k}", to_other_core)
        convs.append(piece(normed, mine, other, of(taps, k), s[0:1]))
    mine = spread(jnp.stack([far_proj[k] for k in hops]), "p", q, c)
    other = send(mine, "dp", to_other_core)
    weights = [w_proj, other_proj]
    for i in range(len(hops)):
        weights += [mine[i], other[i]]
    gain = jnp.concatenate([s[1:2] for s in params])
    shift = jnp.concatenate([s[2:3] for s in params])
    return finish(current, gain, shift, convs, weights)[None]


def local(mesh_shape, *args):
    shard = args[2].shape[0]
    ways, both = mesh_shape["sp"], mesh_shape["tp"]
    if ways == 4 and both == 8 and shard % (16 * ways) == 0 and shard % 128 == 0:
        return fast(*args)
    return plain(*args)


def solution(mesh):
    placed = (
        P("tp", "sp", None),
        P(),
        P("tp", None),
        P("tp", None),
        P(),
        P(),
        P(),
        P(),
        P("tp", None),
    )
    return jax.shard_map(
        functools.partial(local, dict(mesh.shape)),
        mesh=mesh,
        in_specs=placed,
        out_specs=P("tp", "sp", None),
        check_vma=False,
    )
```

time: 153 us -> 107 us (0.70); the launches traced: 151 us -> 106 us
  waiting for transfers between devices: 111 us -> 46.8 us
  starting transfers between devices: 3.15 us -> 26 us
  Pallas kernels: 0 us -> 18.9 us
  between operations: 13.5 us -> 0.64 us
  matrix products: 11.4 us -> 0 us
  local copies, waits for them, and re-layouts: 0.14 us -> 6.46 us
  other arithmetic: 11.4 us -> 7.52 us
    all_gather x2 -> x0, waiting for transfers between devices: 108 us -> none  [the longest x1 80.8 us: local(): lax.all_gather(paired, 'tp', axis=0, tiled=True)]
    ppermute x1 -> x21, waiting for transfers between devices: 2.75 us -> 46.8 us  [send(): return lax.ppermute(value, ('sp', 'tp'), pairs)]
    ppermute x1 -> x21, starting transfers between devices: 3.11 us -> 26 us  [send(): return lax.ppermute(value, ('sp', 'tp'), pairs)]
    pallas_call x0 -> x5, Pallas kernels: none -> 18.9 us  [the longest x4 13.9 us: piece(): pl.pallas_call(piece_kernel, out_shape=jax.ShapeDtypeStruct((rows, lanes)...]
    dot_general x2 -> x0, matrix products: 11.4 us -> none  [the longest x1 5.89 us: local(): jnp.einsum('td,nrd->trn', normed, lax.all_gather(paired, 'tp', axis=0, ti...]
    reduce_sum x1 -> x0, other arithmetic: 7.54 us -> none  [local(): mean = jnp.mean(conv, axis=1, keepdims=True)]
    dynamic_slice x0 -> x2, local copies, waits for them, and re-layouts: none -> 1.58 us  [the longest x1 1.57 us: cut(): return lax.dynamic_slice_in_dim(w, q * quarter, quarter, 0)]
    reduce_sum x1 -> x2, other arithmetic: 0.39 us -> 1.93 us  [rms_rows(): scale = lax.rsqrt(jnp.mean(full * full, axis=1, keepdims=True) + EPS)]
  transfers between devices with their start and end apart: 3 -> 21, of which waited for: 3 -> 9; matrix products, arithmetic and copies ran while one was open for 10% -> 11% of each run, Pallas kernels for 0% -> 13%
where the time goes in v1:
time: 107 us; the launch traced here: 106 us
  waiting for transfers between devices  46.8 us (44%)
  starting transfers between devices  26 us (24%)
  Pallas kernels  18.9 us (18%)
  other arithmetic  7.52 us (7%)
  local copies, waits for them, and re-layouts  6.46 us (6%)
    ppermute x21, waiting for transfers between devices, send(): return lax.ppermute(value, ('sp', 'tp'), pairs)  46.8 us
    ppermute x21, starting transfers between devices, send(): return lax.ppermute(value, ('sp', 'tp'), pairs)  26 us
    pallas_call x4, Pallas kernels, piece(): pl.pallas_call(piece_kernel, out_shape=jax.ShapeDtypeStruct((rows, lanes)...  13.9 us
    pallas_call x1, Pallas kernels, finish(): pl.pallas_call(functools.partial(finish_kernel, len(convs)), out_shape=ja...  5.05 us
  transfers between devices with their start and end apart: 21, of which 9 were waited for; matrix products, arithmetic and copies ran while one was open for 11% of the time, Pallas kernels for 13%

profile of v1, /device:TPU:21, one launch (start us, length us, event | category | flops | bytes accessed | tf_op | source)
XLA Modules:
  0.0 106.4 jit_solution(909553400032718184)
XLA Ops:
  0.0 1.1 %dynamic-slice_bitcast_fusion = (bf16[1,32,2048]{2,1,0:T(8,128)(2,1)S(1)}, bf16[1,32,2048]{2,1,0:T(8,128)(2,1)S(1)}) fusion(bf16[128,2048]{1,0:T(8,128)(2,1)} %param.12, s32[]{:T(128)S(6)} %select_n.82, bf16[128,2048]{1,0:T(8,128)(2,1)} %param.11), kind=kLoop, calls=%fused_computation.33 | loop fusion | bytes 524292 | tf_op jit(solution)/shard_map/stack | solution.py:192
  1.9 1.3 %collective-permute-start.2 = (bf16[2,32,2048]{2,1,0:T(8,128)(2,1)}, bf16[2,32,2048]{2,1,0:T(8,128)(2,1)S(1)}, u32[]{:S(2)}, u32[]{:S(2)}) collective-permute-start(bf16[2,32,2048]{2,1,0:T(8,128)(2,1)} %pad_maximum_fusion.7), channel_id=1, source_target_pairs={{0,2},{1,3},{2,0},{3,1},{4,6},{5,7},{6,4},{7,5},{8,10},{9,11},{10,... | collective-permute-start | bytes 786440 | tf_op jit(solution)/shard_map/zg1/ppermute | solution.py:147
  3.2 1.6 %constant_dynamic-slice_fusion = bf16[32,2048]{1,0:T(8,128)(2,1)} fusion(bf16[128,2048]{1,0:T(8,128)(2,1)} %refs_4_.1, s32[]{:T(128)S(6)} %select_n.82), kind=kLoop, calls=%fused_computation.46 | loop fusion | bytes 262148 | tf_op jit(solution)/shard_map/dynamic_slice | solution.py:189
  4.7 2.2 %collective-permute-start.17 = (bf16[32,2048]{1,0:T(8,128)(2,1)}, bf16[32,2048]{1,0:T(8,128)(2,1)S(1)}, u32[]{:S(2)}, u32[]{:S(2)}) collective-permute-start(bf16[32,2048]{1,0:T(8,128)(2,1)} %constant_dynamic-slice_fusion), channel_id=1, source_target_pairs={{0,4},{1,5},{2,6},{3,7},{4,0},{5,1},{6,2},{7,3},{8,12},{9,13},{10,... | collective-permute-start | bytes 393224 | tf_op jit(solution)/shard_map/zp2/ppermute | solution.py:147
  7.2 1.1 %collective-permute-start.15 = (bf16[32,2048]{1,0:T(8,128)(2,1)}, bf16[32,2048]{1,0:T(8,128)(2,1)}, u32[]{:S(2)}, u32[]{:S(2)}) collective-permute-start(bf16[32,2048]{1,0:T(8,128)(2,1)} %constant_dynamic-slice_fusion), channel_id=1, source_target_pairs={{0,2},{1,3},{2,0},{3,1},{4,6},{5,7},{6,4},{7,5},{8,10},{9,11},{10,... | collective-permute-start | bytes 393224 | tf_op jit(solution)/shard_map/zp1/ppermute | solution.py:147
  8.3 1.8 %fusion = f32[384]{0:T(512)S(1)} fusion(bf16[1,384,2048]{2,1,0:T(8,128)(2,1)} %param.9), kind=kLoop, calls=%fused_computation.2 | loop fusion | flops 2358912 | bytes 1574400 | tf_op jit(solution)/shard_map/reduce_sum | solution.py:21
  11.1 1.6 %fusion.2 = bf16[384,2048]{1,0:T(8,128)(2,1)} fusion(f32[2048]{0:T(1024)S(1)} %copy-done.6, f32[384]{0:T(512)S(1)} %add_rsqrt_fusion, bf16[1,384,2048]{2,1,0:T(8,128)(2,1)S(1)} %copy-done), kind=kLoop, calls=%fused_computation.4 | loop fusion | flops 3145728 | bytes 3155456 | tf_op jit(solution)/shard_map/convert_element_type | solution.py:22
  13.6 0.8 dynamic-slice_bitcast_fusion.2
  14.4 8.0 %collective-permute-done.17 = bf16[32,2048]{1,0:T(8,128)(2,1)S(1)} collective-permute-done((bf16[32,2048]{1,0:T(8,128)(2,1)}, bf16[32,2048]{1,0:T(8,128)(2,1)S(1)}, u32[]{:S(2)}, u32[]{:S(2)}) %collective-permute-start.17) | collective-permute-done | bytes 131104 | tf_op jit(solution)/shard_map/zp2/ppermute | solution.py:147
  22.4 3.1 %collective-permute-start.10 = (bf16[2,32,2048]{2,1,0:T(8,128)(2,1)}, bf16[2,32,2048]{2,1,0:T(8,128)(2,1)S(1)}, u32[]{:S(2)}, u32[]{:S(2)}) collective-permute-start(bf16[2,32,2048]{2,1,0:T(8,128)(2,1)} %pad_maximum_fusion.7), channel_id=1, source_target_pairs={{0,4},{1,5},{2,6},{3,7},{4,0},{5,1},{6,2},{7,3},{8,12},{9,13},{10,... | collective-permute-start | bytes 786440 | tf_op jit(solution)/shard_map/zg2/ppermute | solution.py:147
  25.6 7.1 %collective-permute-done.16 = bf16[32,2048]{1,0:T(8,128)(2,1)} collective-permute-done((bf16[32,2048]{1,0:T(8,128)(2,1)}, bf16[32,2048]{1,0:T(8,128)(2,1)}, u32[]{:S(2)}, u32[]{:S(2)}) %collective-permute-start.16) | collective-permute-done | bytes 131104 | tf_op jit(solution)/shard_map/zp3/ppermute | solution.py:147
  32.7 3.1 %collective-permute-start = (bf16[32,2048]{1,0:T(8,128)(2,1)}, bf16[32,2048]{1,0:T(8,128)(2,1)S(1)}, u32[]{:S(2)}, u32[]{:S(2)}) collective-permute-start(bf16[32,2048]{1,0:T(8,128)(2,1)} %slice_bitcast_fusion.6), channel_id=1, source_target_pairs={{0,8},{1,9},{2,10},{3,11},{4,12},{5,13},{6,14},{7,15},{8,16},{9,17... | collective-permute-start | bytes 393224 | tf_op jit(solution)/shard_map/halo/ppermute | solution.py:147
  35.8 3.8 %collective-permute-start.1 = (bf16[2,128,2048]{2,1,0:T(8,128)(2,1)S(1)}, bf16[2,128,2048]{2,1,0:T(8,128)(2,1)S(1)}, u32[]{:S(2)}, u32[]{:S(2)}) collective-permute-start(bf16[2,128,2048]{2,1,0:T(8,128)(2,1)S(1)} %pad_maximum_fusion.1.mine), channel_id=1, source_target_pairs={{0,1},{1,0},{2,3},{3,2},{4,5},{5,4},{6,7},{7,6},{8,9},{9,8},{10,11... | collective-permute-start | bytes 3145736 | tf_op jit(solution)/shard_map/dg0/ppermute | solution.py:147
  39.7 1.1 pad_maximum_fusion.6
  41.3 1.2 %collective-permute-start.3 = (bf16[2,32,2048]{2,1,0:T(8,128)(2,1)S(1)}, bf16[2,32,2048]{2,1,0:T(8,128)(2,1)S(1)}, u32[]{:S(2)}, u32[]{:S(2)}) collective-permute-start(bf16[2,32,2048]{2,1,0:T(8,128)(2,1)S(1)} %collective-permute-done.2), channel_id=1, source_target_pairs={{0,8},{1,17},{2,10},{3,19},{4,12},{5,21},{6,14},{7,23},{8,0},{9,25... | collective-permute-start | bytes 786440 | tf_op jit(solution)/shard_map/xag1/ppermute | solution.py:147
  43.1 1.3 %collective-permute-start.11 = (bf16[2,32,2048]{2,1,0:T(8,128)(2,1)S(1)}, bf16[2,32,2048]{2,1,0:T(8,128)(2,1)S(1)}, u32[]{:S(2)}, u32[]{:S(2)}) collective-permute-start(bf16[2,32,2048]{2,1,0:T(8,128)(2,1)S(1)} %collective-permute-done.10), channel_id=1, source_target_pairs={{0,8},{1,17},{2,10},{3,19},{4,12},{5,21},{6,14},{7,23},{8,0},{9,25... | collective-permute-start | bytes 786440 | tf_op jit(solution)/shard_map/xag2/ppermute | solution.py:147
  44.6 6.2 %collective-permute-done.3 = bf16[2,32,2048]{2,1,0:T(8,128)(2,1)S(1)} collective-permute-done((bf16[2,32,2048]{2,1,0:T(8,128)(2,1)S(1)}, bf16[2,32,2048]{2,1,0:T(8,128)(2,1)S(1)}, u32[]{:S(2)}, u32[]{:S(2)}) %collective-permute-start.3) | collective-permute-done | bytes 262176 | tf_op jit(solution)/shard_map/xag1/ppermute | solution.py:147
  50.9 2.7 %collective-permute-done.7 = bf16[2,32,2048]{2,1,0:T(8,128)(2,1)S(1)} collective-permute-done((bf16[2,32,2048]{2,1,0:T(8,128)(2,1)S(1)}, bf16[2,32,2048]{2,1,0:T(8,128)(2,1)S(1)}, u32[]{:S(2)}, u32[]{:S(2)}) %collective-permute-start.7) | collective-permute-done | bytes 262176 | tf_op jit(solution)/shard_map/xag3/ppermute | solution.py:147
  53.7 2.7 %collective-permute-done.11 = bf16[2,32,2048]{2,1,0:T(8,128)(2,1)S(1)} collective-permute-done((bf16[2,32,2048]{2,1,0:T(8,128)(2,1)S(1)}, bf16[2,32,2048]{2,1,0:T(8,128)(2,1)S(1)}, u32[]{:S(2)}, u32[]{:S(2)}) %collective-permute-start.11) | collective-permute-done | bytes 262176 | tf_op jit(solution)/shard_map/xag2/ppermute | solution.py:147
  56.5 1.0 pad_maximum_fusion.2
  57.5 1.5 %collective-permute-start.19 = (bf16[3,64,2048]{2,1,0:T(8,128)(2,1)S(1)}, bf16[3,64,2048]{2,1,0:T(8,128)(2,1)S(1)}, u32[]{:S(2)}, u32[]{:S(2)}) collective-permute-start(bf16[3,64,2048]{2,1,0:T(8,128)(2,1)S(1)} %pad_maximum_fusion.2), channel_id=1, source_target_pairs={{0,16},{1,9},{2,18},{3,11},{4,20},{5,13},{6,22},{7,15},{8,24},{9,1... | collective-permute-start | bytes 2359304 | tf_op jit(solution)/shard_map/xbp/ppermute | solution.py:147
  59.2 5.6 %collective-permute-done.4 = bf16[2,64,2048]{2,1,0:T(8,128)(2,1)S(1)} collective-permute-done((bf16[2,64,2048]{2,1,0:T(8,128)(2,1)S(1)}, bf16[2,64,2048]{2,1,0:T(8,128)(2,1)S(1)}, u32[]{:S(2)}, u32[]{:S(2)}) %collective-permute-start.4) | collective-permute-done | bytes 524320 | tf_op jit(solution)/shard_map/xbg1/ppermute | solution.py:147
  64.9 5.6 %collective-permute-start.5 = (bf16[2,128,2048]{2,1,0:T(8,128)(2,1)S(1)}, bf16[2,128,2048]{2,1,0:T(8,128)(2,1)S(1)}, u32[]{:S(2)}, u32[]{:S(2)}) collective-permute-start(bf16[2,128,2048]{2,1,0:T(8,128)(2,1)S(1)} %slice_dynamic-update-slice_fusion.6.mine), channel_id=1, source_target_pairs={{0,1},{1,0},{2,3},{3,2},{4,5},{5,4},{6,7},{7,6},{8,9},{9,8},{10,11... | collective-permute-start | bytes 3145736 | tf_op jit(solution)/shard_map/dg1/ppermute | solution.py:147
  70.4 0.9 collective-permute-done.8
  71.4 5.5 %collective-permute-done.12 = bf16[2,64,2048]{2,1,0:T(8,128)(2,1)S(1)} collective-permute-done((bf16[2,64,2048]{2,1,0:T(8,128)(2,1)S(1)}, bf16[2,64,2048]{2,1,0:T(8,128)(2,1)S(1)}, u32[]{:S(2)}, u32[]{:S(2)}) %collective-permute-start.12) | collective-permute-done | bytes 524320 | tf_op jit(solution)/shard_map/xbg2/ppermute | solution.py:147
  76.9 8.1 %collective-permute-done.19 = bf16[3,64,2048]{2,1,0:T(8,128)(2,1)S(1)} collective-permute-done((bf16[3,64,2048]{2,1,0:T(8,128)(2,1)S(1)}, bf16[3,64,2048]{2,1,0:T(8,128)(2,1)S(1)}, u32[]{:S(2)}, u32[]{:S(2)}) %collective-permute-start.19) | collective-permute-done | bytes 786464 | tf_op jit(solution)/shard_map/xbp/ppermute | solution.py:147
  86.1 0.8 copy-done.1
  87.0 3.4 %shard_map.91.refs_0_ = f32[384,256]{1,0:T(8,128)S(1)} custom-call(bf16[416,2048]{1,0:T(8,128)(2,1)S(1)} %pad_maximum_fusion.normed, bf16[2,128,2048]{2,1,0:T(8,128)(2,1)S(1)} %pad_maximum_fusion.1.mine, bf16[2,128,2048]{2,1,0:T(8,128)(2,1)S(1)} %collective-permute-done.1.other, f32[31,256]{1,0:T(8,128)S(1)} %get-tuple-element.16.taps, ...), custom_call_target="tpu_custom_call" | custom-call | flops 872415232 | tf_op jit(solution)/shard_map/pallas_call | solution.py:91
  90.6 3.4 %shard_map.92.refs_1_ = f32[384,256]{1,0:T(8,128)S(1)} custom-call(bf16[416,2048]{1,0:T(8,128)(2,1)S(1)} %pad_maximum_fusion.normed, bf16[2,128,2048]{2,1,0:T(8,128)(2,1)S(1)} %slice_dynamic-update-slice_fusion.6.mine, bf16[2,128,2048]{2,1,0:T(8,128)(2,1)S(1)} %collective-permute-done.5.other, f32[31,256]{1,0:T(8,128)S(1)} %get-tuple-element.15.taps, ...), custom_call_target="tpu_custom_call" | custom-call | flops 872415232 | tf_op jit(solution)/shard_map/pallas_call | solution.py:91
  94.0 3.4 %shard_map.93.refs_2_ = f32[384,256]{1,0:T(8,128)S(1)} custom-call(bf16[416,2048]{1,0:T(8,128)(2,1)S(1)} %pad_maximum_fusion.normed, bf16[2,128,2048]{2,1,0:T(8,128)(2,1)S(1)} %slice_dynamic-update-slice_fusion.4.mine, bf16[2,128,2048]{2,1,0:T(8,128)(2,1)S(1)} %collective-permute-done.9.other, f32[31,256]{1,0:T(8,128)S(1)} %get-tuple-element.14.taps, ...), custom_call_target="tpu_custom_call" | custom-call | flops 872415232 | tf_op jit(solution)/shard_map/pallas_call | solution.py:91
  97.5 3.6 %shard_map.94.refs_3_ = f32[384,256]{1,0:T(8,128)S(1)} custom-call(bf16[416,2048]{1,0:T(8,128)(2,1)S(1)} %pad_maximum_fusion.normed, bf16[2,128,2048]{2,1,0:T(8,128)(2,1)S(1)} %slice_dynamic-update-slice_fusion.2.mine, bf16[2,128,2048]{2,1,0:T(8,128)(2,1)S(1)} %collective-permute-done.13.other, f32[31,256]{1,0:T(8,128)S(1)} %get-tuple-element.13.taps, ...), custom_call_target="tpu_custom_call" | custom-call | flops 872415232 | tf_op jit(solution)/shard_map/pallas_call | solution.py:91
  101.3 5.1 %shard_map.95 = bf16[384,2048]{1,0:T(8,128)(2,1)} custom-call(bf16[384,2048]{1,0:T(8,128)(2,1)S(1)} %bitcast.67, f32[4,256]{1,0:T(4,128)S(1)} %get-tuple-element.37.gain, f32[4,256]{1,0:T(4,128)S(1)} %get-tuple-element.38.shift, f32[384,256]{1,0:T(8,128)S(1)} %shard_map.91.refs_0_, f32[384,256]{1,0:T(8,128)S(1)} %shard_map.92.refs_1_, ...), custom_call_target="tpu_custom_call" | custom-call | flops 1610612736 | tf_op jit(solution)/shard_map/pallas_call | solution.py:125
  (93 shorter events, 5.9 us)
Async XLA Ops:
  0.0 10.1 %copy-start = (bf16[1,384,2048]{2,1,0:T(8,128)(2,1)S(1)}, bf16[1,384,2048]{2,1,0:T(8,128)(2,1)}, u32[]{:S(2)}) copy-start(bf16[1,384,2048]{2,1,0:T(8,128)(2,1)} %param.9) | copy-start | bytes 4718596
  0.0 10.7 %copy-start.7 = (f32[1024]{0:T(1024)S(1)}, f32[1024]{0:T(1024)}, u32[]{:S(2)}) copy-start(f32[1024]{0:T(1024)} %param.14) | copy-start | bytes 12292
  0.0 10.8 %copy-start.8 = (f32[1024]{0:T(1024)S(1)}, f32[1024]{0:T(1024)}, u32[]{:S(2)}) copy-start(f32[1024]{0:T(1024)} %param.15) | copy-start | bytes 12292
  0.0 10.8 %copy-start.9 = (f32[1024]{0:T(1024)S(1)}, f32[1024]{0:T(1024)}, u32[]{:S(2)}) copy-start(f32[1024]{0:T(1024)} %param.16) | copy-start | bytes 12292
  0.0 11.0 %copy-start.5 = (bf16[31,1024]{1,0:T(8,128)(2,1)S(1)}, bf16[31,1024]{1,0:T(8,128)(2,1)}, u32[]{:S(2)}) copy-start(bf16[31,1024]{1,0:T(8,128)(2,1)} %param.13) | copy-start | bytes 190468
  1.9 9.2 %copy-start.6 = (f32[2048]{0:T(1024)S(1)}, f32[2048]{0:T(1024)}, u32[]{:S(2)}) copy-start(f32[2048]{0:T(1024)} %param.10) | copy-start | bytes 24580
  1.9 39.4 %collective-permute-start.2 = (bf16[2,32,2048]{2,1,0:T(8,128)(2,1)}, bf16[2,32,2048]{2,1,0:T(8,128)(2,1)S(1)}, u32[]{:S(2)}, u32[]{:S(2)}) collective-permute-start(bf16[2,32,2048]{2,1,0:T(8,128)(2,1)} %pad_maximum_fusion.7), channel_id=1, source_target_pairs={{0,2},{1,3},{2,0},{3,1},{4,6},{5,7},{6,4},{7,5},{8,10},{9,11},{10,... | collective-permute-start | bytes 786440 | tf_op jit(solution)/shard_map/zg1/ppermute | solution.py:147
  3.2 39.5 %collective-permute-start.6 = (bf16[2,32,2048]{2,1,0:T(8,128)(2,1)}, bf16[2,32,2048]{2,1,0:T(8,128)(2,1)S(1)}, u32[]{:S(2)}, u32[]{:S(2)}) collective-permute-start(bf16[2,32,2048]{2,1,0:T(8,128)(2,1)} %pad_maximum_fusion.7), channel_id=1, source_target_pairs={{0,6},{1,7},{2,4},{3,5},{4,2},{5,3},{6,0},{7,1},{8,14},{9,15},{10,... | collective-permute-start | bytes 786440 | tf_op jit(solution)/shard_map/zg3/ppermute | solution.py:147
  4.7 17.7 %collective-permute-start.17 = (bf16[32,2048]{1,0:T(8,128)(2,1)}, bf16[32,2048]{1,0:T(8,128)(2,1)S(1)}, u32[]{:S(2)}, u32[]{:S(2)}) collective-permute-start(bf16[32,2048]{1,0:T(8,128)(2,1)} %constant_dynamic-slice_fusion), channel_id=1, source_target_pairs={{0,4},{1,5},{2,6},{3,7},{4,0},{5,1},{6,2},{7,3},{8,12},{9,13},{10,... | collective-permute-start | bytes 393224 | tf_op jit(solution)/shard_map/zp2/ppermute | solution.py:147
  7.0 25.7 %collective-permute-start.16 = (bf16[32,2048]{1,0:T(8,128)(2,1)}, bf16[32,2048]{1,0:T(8,128)(2,1)}, u32[]{:S(2)}, u32[]{:S(2)}) collective-permute-start(bf16[32,2048]{1,0:T(8,128)(2,1)} %constant_dynamic-slice_fusion), channel_id=1, source_target_pairs={{0,6},{1,7},{2,4},{3,5},{4,2},{5,3},{6,0},{7,1},{8,14},{9,15},{10,... | collective-permute-start | bytes 393224 | tf_op jit(solution)/shard_map/zp3/ppermute | solution.py:147
  7.2 28.6 %collective-permute-start.15 = (bf16[32,2048]{1,0:T(8,128)(2,1)}, bf16[32,2048]{1,0:T(8,128)(2,1)}, u32[]{:S(2)}, u32[]{:S(2)}) collective-permute-start(bf16[32,2048]{1,0:T(8,128)(2,1)} %constant_dynamic-slice_fusion), channel_id=1, source_target_pairs={{0,2},{1,3},{2,0},{3,1},{4,6},{5,7},{6,4},{7,5},{8,10},{9,11},{10,... | collective-permute-start | bytes 393224 | tf_op jit(solution)/shard_map/zp1/ppermute | solution.py:147
  11.1 1.6 %copy-start.3 = (bf16[128,2048]{1,0:T(8,128)(2,1)S(1)}, bf16[128,2048]{1,0:T(8,128)(2,1)}, u32[]{:S(2)}) copy-start(bf16[128,2048]{1,0:T(8,128)(2,1)} %param.12) | copy-start | bytes 1572868
  11.1 1.6 %copy-start.4 = (bf16[128,2048]{1,0:T(8,128)(2,1)S(1)}, bf16[128,2048]{1,0:T(8,128)(2,1)}, u32[]{:S(2)}) copy-start(bf16[128,2048]{1,0:T(8,128)(2,1)} %param.11) | copy-start | bytes 1572868
  22.4 20.7 %collective-permute-start.10 = (bf16[2,32,2048]{2,1,0:T(8,128)(2,1)}, bf16[2,32,2048]{2,1,0:T(8,128)(2,1)S(1)}, u32[]{:S(2)}, u32[]{:S(2)}) collective-permute-start(bf16[2,32,2048]{2,1,0:T(8,128)(2,1)} %pad_maximum_fusion.7), channel_id=1, source_target_pairs={{0,4},{1,5},{2,6},{3,7},{4,0},{5,1},{6,2},{7,3},{8,12},{9,13},{10,... | collective-permute-start | bytes 786440 | tf_op jit(solution)/shard_map/zg2/ppermute | solution.py:147
  32.7 8.1 %collective-permute-start = (bf16[32,2048]{1,0:T(8,128)(2,1)}, bf16[32,2048]{1,0:T(8,128)(2,1)S(1)}, u32[]{:S(2)}, u32[]{:S(2)}) collective-permute-start(bf16[32,2048]{1,0:T(8,128)(2,1)} %slice_bitcast_fusion.6), channel_id=1, source_target_pairs={{0,8},{1,9},{2,10},{3,11},{4,12},{5,13},{6,14},{7,15},{8,16},{9,17... | collective-permute-start | bytes 393224 | tf_op jit(solution)/shard_map/halo/ppermute | solution.py:147
  35.8 50.3 %collective-permute-start.1 = (bf16[2,128,2048]{2,1,0:T(8,128)(2,1)S(1)}, bf16[2,128,2048]{2,1,0:T(8,128)(2,1)S(1)}, u32[]{:S(2)}, u32[]{:S(2)}) collective-permute-start(bf16[2,128,2048]{2,1,0:T(8,128)(2,1)S(1)} %pad_maximum_fusion.1.mine), channel_id=1, source_target_pairs={{0,1},{1,0},{2,3},{3,2},{4,5},{5,4},{6,7},{7,6},{8,9},{9,8},{10,11... | collective-permute-start | bytes 3145736 | tf_op jit(solution)/shard_map/dg0/ppermute | solution.py:147
  41.0 15.5 %collective-permute-start.18 = (bf16[3,32,2048]{2,1,0:T(8,128)(2,1)S(1)}, bf16[3,32,2048]{2,1,0:T(8,128)(2,1)S(1)}, u32[]{:S(2)}, u32[]{:S(2)}) collective-permute-start(bf16[3,32,2048]{2,1,0:T(8,128)(2,1)S(1)} %get-tuple-element.11), channel_id=1, source_target_pairs={{0,8},{1,17},{2,10},{3,19},{4,12},{5,21},{6,14},{7,23},{8,0},{9,25... | collective-permute-start | bytes 1179656 | tf_op jit(solution)/shard_map/xap/ppermute | solution.py:147
  41.3 9.5 %collective-permute-start.3 = (bf16[2,32,2048]{2,1,0:T(8,128)(2,1)S(1)}, bf16[2,32,2048]{2,1,0:T(8,128)(2,1)S(1)}, u32[]{:S(2)}, u32[]{:S(2)}) collective-permute-start(bf16[2,32,2048]{2,1,0:T(8,128)(2,1)S(1)} %collective-permute-done.2), channel_id=1, source_target_pairs={{0,8},{1,17},{2,10},{3,19},{4,12},{5,21},{6,14},{7,23},{8,0},{9,25... | collective-permute-start | bytes 786440 | tf_op jit(solution)/shard_map/xag1/ppermute | solution.py:147
  42.7 10.9 %collective-permute-start.7 = (bf16[2,32,2048]{2,1,0:T(8,128)(2,1)S(1)}, bf16[2,32,2048]{2,1,0:T(8,128)(2,1)S(1)}, u32[]{:S(2)}, u32[]{:S(2)}) collective-permute-start(bf16[2,32,2048]{2,1,0:T(8,128)(2,1)S(1)} %collective-permute-done.6), channel_id=1, source_target_pairs={{0,8},{1,17},{2,10},{3,19},{4,12},{5,21},{6,14},{7,23},{8,0},{9,25... | collective-permute-start | bytes 786440 | tf_op jit(solution)/shard_map/xag3/ppermute | solution.py:147
  43.1 13.3 %collective-permute-start.11 = (bf16[2,32,2048]{2,1,0:T(8,128)(2,1)S(1)}, bf16[2,32,2048]{2,1,0:T(8,128)(2,1)S(1)}, u32[]{:S(2)}, u32[]{:S(2)}) collective-permute-start(bf16[2,32,2048]{2,1,0:T(8,128)(2,1)S(1)} %collective-permute-done.10), channel_id=1, source_target_pairs={{0,8},{1,17},{2,10},{3,19},{4,12},{5,21},{6,14},{7,23},{8,0},{9,25... | collective-permute-start | bytes 786440 | tf_op jit(solution)/shard_map/xag2/ppermute | solution.py:147
  50.8 14.0 %collective-permute-start.4 = (bf16[2,64,2048]{2,1,0:T(8,128)(2,1)S(1)}, bf16[2,64,2048]{2,1,0:T(8,128)(2,1)S(1)}, u32[]{:S(2)}, u32[]{:S(2)}) collective-permute-start(bf16[2,64,2048]{2,1,0:T(8,128)(2,1)S(1)} %pad_maximum_fusion.3), channel_id=1, source_target_pairs={{0,16},{1,9},{2,18},{3,11},{4,20},{5,13},{6,22},{7,15},{8,24},{9,1... | collective-permute-start | bytes 1572872 | tf_op jit(solution)/shard_map/xbg1/ppermute | solution.py:147
  53.6 17.7 %collective-permute-start.8 = (bf16[2,64,2048]{2,1,0:T(8,128)(2,1)S(1)}, bf16[2,64,2048]{2,1,0:T(8,128)(2,1)S(1)}, u32[]{:S(2)}, u32[]{:S(2)}) collective-permute-start(bf16[2,64,2048]{2,1,0:T(8,128)(2,1)S(1)} %pad_maximum_fusion.4), channel_id=1, source_target_pairs={{0,16},{1,9},{2,18},{3,11},{4,20},{5,13},{6,22},{7,15},{8,24},{9,1... | collective-permute-start | bytes 1572872 | tf_op jit(solution)/shard_map/xbg3/ppermute | solution.py:147
  56.4 20.5 %collective-permute-start.12 = (bf16[2,64,2048]{2,1,0:T(8,128)(2,1)S(1)}, bf16[2,64,2048]{2,1,0:T(8,128)(2,1)S(1)}, u32[]{:S(2)}, u32[]{:S(2)}) collective-permute-start(bf16[2,64,2048]{2,1,0:T(8,128)(2,1)S(1)} %pad_maximum_fusion.5), channel_id=1, source_target_pairs={{0,16},{1,9},{2,18},{3,11},{4,20},{5,13},{6,22},{7,15},{8,24},{9,1... | collective-permute-start | bytes 1572872 | tf_op jit(solution)/shard_map/xbg2/ppermute | solution.py:147
  57.5 27.5 %collective-permute-start.19 = (bf16[3,64,2048]{2,1,0:T(8,128)(2,1)S(1)}, bf16[3,64,2048]{2,1,0:T(8,128)(2,1)S(1)}, u32[]{:S(2)}, u32[]{:S(2)}) collective-permute-start(bf16[3,64,2048]{2,1,0:T(8,128)(2,1)S(1)} %pad_maximum_fusion.2), channel_id=1, source_target_pairs={{0,16},{1,9},{2,18},{3,11},{4,20},{5,13},{6,22},{7,15},{8,24},{9,1... | collective-permute-start | bytes 2359304 | tf_op jit(solution)/shard_map/xbp/ppermute | solution.py:147
  64.9 25.7 %collective-permute-start.5 = (bf16[2,128,2048]{2,1,0:T(8,128)(2,1)S(1)}, bf16[2,128,2048]{2,1,0:T(8,128)(2,1)S(1)}, u32[]{:S(2)}, u32[]{:S(2)}) collective-permute-start(bf16[2,128,2048]{2,1,0:T(8,128)(2,1)S(1)} %slice_dynamic-update-slice_fusion.6.mine), channel_id=1, source_target_pairs={{0,1},{1,0},{2,3},{3,2},{4,5},{5,4},{6,7},{7,6},{8,9},{9,8},{10,11... | collective-permute-start | bytes 3145736 | tf_op jit(solution)/shard_map/dg1/ppermute | solution.py:147
  71.4 14.6 %copy-start.2 = (bf16[384,2048]{1,0:T(8,128)(2,1)S(1)}, bf16[384,2048]{1,0:T(8,128)(2,1)}, u32[]{:S(2)}) copy-start(bf16[384,2048]{1,0:T(8,128)(2,1)} %fusion.2) | copy-start | bytes 4718596
  71.4 22.7 %collective-permute-start.9 = (bf16[2,128,2048]{2,1,0:T(8,128)(2,1)S(1)}, bf16[2,128,2048]{2,1,0:T(8,128)(2,1)S(1)}, u32[]{:S(2)}, u32[]{:S(2)}) collective-permute-start(bf16[2,128,2048]{2,1,0:T(8,128)(2,1)S(1)} %slice_dynamic-update-slice_fusion.4.mine), channel_id=1, source_target_pairs={{0,1},{1,0},{2,3},{3,2},{4,5},{5,4},{6,7},{7,6},{8,9},{9,8},{10,11... | collective-permute-start | bytes 3145736 | tf_op jit(solution)/shard_map/dg3/ppermute | solution.py:147
  85.1 16.0 %collective-permute-start.20 = (bf16[3,128,2048]{2,1,0:T(8,128)(2,1)S(1)}, bf16[3,128,2048]{2,1,0:T(8,128)(2,1)S(1)}, u32[]{:S(2)}, u32[]{:S(2)}) collective-permute-start(bf16[3,128,2048]{2,1,0:T(8,128)(2,1)S(1)} %slice_dynamic-update-slice_fusion), channel_id=1, source_target_pairs={{0,1},{1,0},{2,3},{3,2},{4,5},{5,4},{6,7},{7,6},{8,9},{9,8},{10,11... | collective-permute-start | bytes 4718600 | tf_op jit(solution)/shard_map/dp/ppermute | solution.py:147
  85.3 12.2 %collective-permute-start.13 = (bf16[2,128,2048]{2,1,0:T(8,128)(2,1)S(1)}, bf16[2,128,2048]{2,1,0:T(8,128)(2,1)S(1)}, u32[]{:S(2)}, u32[]{:S(2)}) collective-permute-start(bf16[2,128,2048]{2,1,0:T(8,128)(2,1)S(1)} %slice_dynamic-update-slice_fusion.2.mine), channel_id=1, source_target_pairs={{0,1},{1,0},{2,3},{3,2},{4,5},{5,4},{6,7},{7,6},{8,9},{9,8},{10,11... | collective-permute-start | bytes 3145736 | tf_op jit(solution)/shard_map/dg2/ppermute | solution.py:147
  85.9 1.0 copy-start.1
  87.0 14.3 %collective-permute-start.14 = (bf16[128,2048]{1,0:T(8,128)(2,1)S(1)}, bf16[128,2048]{1,0:T(8,128)(2,1)S(1)}, u32[]{:S(2)}, u32[]{:S(2)}) collective-permute-start(bf16[128,2048]{1,0:T(8,128)(2,1)S(1)} %copy-done.1), channel_id=1, source_target_pairs={{0,1},{1,0},{2,3},{3,2},{4,5},{5,4},{6,7},{7,6},{8,9},{9,8},{10,11... | collective-permute-start | bytes 1572872 | tf_op jit(solution)/shard_map/dp0/ppermute | solution.py:147
